TPU v7x, 32 devices: a whole 2x2x4 slice. The times are simulated.
32 devices in a mesh: grp: 2 (over y), kv: 4 (over z), tp: 4 (over x, core).
Axes of the slice: x: 2, y: 2, z: 4, core: 2. Of those that a mesh axis runs over, the one named last changes fastest.
Arguments:
- piece_tokens: bfloat16 [2048, 2048], P(('grp', 'kv')), parts along dimension 0, may hold values from -6 to 6
- dec_tokens: bfloat16 [32, 2048], P(('grp', 'kv')), parts along dimension 0, may hold values from -6 to 6
- norm_gain: float32 [2048], replicated, may hold values from 0.1 to 1.9
- query_weight: bfloat16 [2048, 1024], P(None, 'tp'), may hold values from -0.125 to 0.125
- key_weight: bfloat16 [2048, 1024], P(None, 'tp'), may hold values from -0.125 to 0.125
- value_weight: bfloat16 [2048, 1024], P(None, 'tp'), may hold values from -0.125 to 0.125
- forget_weight: bfloat16 [2048, 8], P(None, 'tp'), may hold values from -0.125 to 0.125
- forget_bias: float32 [8], P('tp'), may hold values from 3 to 13
- out_weight: bfloat16 [1024, 2048], P(None, 'tp'), may hold values from -0.1875 to 0.1875
- cache_keys: bfloat16 [32768, 1024], P(('grp', 'kv'), 'tp'), parts along dimension 0, may hold values from -480 to 480
- cache_values: bfloat16 [32768, 1024], P(('grp', 'kv'), 'tp'), parts along dimension 0, may hold values from -6 to 6
- cache_gates: float32 [8, 32768], P('tp', ('grp', 'kv')), parts along dimension 1, as said below
- dec_keys: bfloat16 [32, 2048, 1024], P(('grp', 'kv'), None, 'tp'), parts along dimension 0, may hold values from -480 to 480
- dec_values: bfloat16 [32, 2048, 1024], P(('grp', 'kv'), None, 'tp'), parts along dimension 0, may hold values from -6 to 6
- dec_gates: float32 [32, 8, 2048], P(('grp', 'kv'), 'tp'), parts along dimension 0, as said below
- dec_lengths: int32 [32], P(('grp', 'kv')), parts along dimension 0, may hold values from 1 to 2048, as said below
Outputs:
- piece_out: bfloat16 [2048, 2048], P(('grp', 'kv'), 'tp'), parts along dimension 0
- dec_out: bfloat16 [32, 2048], P(('grp', 'kv'), 'tp'), parts along dimension 0
- piece_keys: bfloat16 [2048, 1024], P(('grp', 'kv'), 'tp'), parts along dimension 0
- piece_values: bfloat16 [2048, 1024], P(('grp', 'kv'), 'tp'), parts along dimension 0
There are 2 independent parts, one for each index of `grp`. A program takes and returns all parts, laid end to end along the dimension named above; an argument that names none is the same for every part. Nothing has to cross between parts.
Inputs may be any that keep to these rules, and one draw needn't show every extreme that they name: cache_gates never falls along positions and is 0 at the last cached position. dec_gates never falls along a sequence's live slots and is 0 at its last live slot and beyond. Slots 0 to dec_lengths[b] - 1 of sequence b are live; some sequence has exactly 2048.
All inputs are finite; a program needn't handle non-finite values.
Results may differ from a plain program's by a relative error of at most 0.015.
Values may be sent and summed in bfloat16 or wider, within the bound.
A program may use at most 128 MiB of HBM per device.

v0:
```python
import math

import jax
import jax.numpy as jnp
from jax import lax
from jax.sharding import PartitionSpec as P

norm_eps = 1e-05


def carried_in(part, axis, combine, identity):
    place = lax.axis_index(axis)
    gathered = lax.all_gather(part, axis)
    state = jnp.zeros_like(part) + jnp.asarray(identity, part.dtype)

    def one(lap, state):
        return combine(state, lax.dynamic_index_in_dim(gathered, lap, 0, False))

    return lax.fori_loop(0, place, one, state)


def rms_norm(tokens, norm_gain):
    values = tokens.astype(jnp.float32)
    factor = lax.rsqrt(jnp.mean(values * values, axis=-1, keepdims=True) + norm_eps)
    return (values * factor * norm_gain).astype(jnp.bfloat16)


def project(tokens, norm_gain, query_weight, key_weight, value_weight, forget_weight, forget_bias):
    normed = rms_norm(tokens, norm_gain)
    queries = jnp.dot(normed, query_weight, preferred_element_type=jnp.float32).astype(jnp.bfloat16)
    key_rows = jnp.dot(normed, key_weight, preferred_element_type=jnp.float32).astype(jnp.bfloat16)
    value_rows = jnp.dot(normed, value_weight, preferred_element_type=jnp.float32).astype(
        jnp.bfloat16
    )
    log_gates = jax.nn.log_sigmoid(
        jnp.dot(normed, forget_weight, preferred_element_type=jnp.float32) + forget_bias
    )
    return (queries, key_rows, value_rows, log_gates)


def add_pair(earlier_sum, later_sum):
    return earlier_sum + later_sum


def shards(
    piece_tokens,
    dec_tokens,
    norm_gain,
    query_weight,
    key_weight,
    value_weight,
    forget_weight,
    forget_bias,
    out_weight,
    cache_keys,
    cache_values,
    cache_gates,
    dec_keys,
    dec_values,
    dec_gates,
    dec_lengths,
):
    piece_count = piece_tokens.shape[0]
    local_heads = forget_weight.shape[1]
    head_size = query_weight.shape[1] // local_heads
    score_scale = head_size ** (-0.5)
    piece_parts = project(
        piece_tokens, norm_gain, query_weight, key_weight, value_weight, forget_weight, forget_bias
    )
    dec_parts = project(
        dec_tokens, norm_gain, query_weight, key_weight, value_weight, forget_weight, forget_bias
    )
    piece_queries, piece_keys, piece_values, piece_gates = piece_parts
    dec_queries, dec_new_keys, dec_new_values, dec_gate_now = dec_parts
    running = jnp.cumsum(piece_gates, axis=0)
    offset = carried_in(running[-1], "kv", add_pair, jnp.zeros_like(running[-1]))
    piece_bias = -(running + offset[None, :]).T
    all_queries = lax.all_gather(piece_queries, "kv", axis=0, tiled=True)
    shard_index = lax.axis_index("kv")
    key_order = shard_index * piece_count + jnp.arange(piece_count, dtype=jnp.int32)
    cache_rows = cache_keys.shape[0]
    cache_key_heads = cache_keys.reshape(cache_rows, local_heads, head_size)
    cache_value_heads = cache_values.reshape(cache_rows, local_heads, head_size)
    piece_key_heads = piece_keys.reshape(piece_count, local_heads, head_size)
    piece_value_heads = piece_values.reshape(piece_count, local_heads, head_size)
    total_rows = all_queries.shape[0]
    block_rows = math.gcd(total_rows, 512)
    block_count = total_rows // block_rows
    query_blocks = all_queries.reshape(block_count, block_rows, local_heads, head_size)
    block_starts = jnp.arange(block_count, dtype=jnp.int32) * block_rows

    def block_terms(inputs):
        query_block, first_row = inputs
        cache_scores = (
            jnp.einsum(
                "qhd,khd->hqk", query_block, cache_key_heads, preferred_element_type=jnp.float32
            )
            * score_scale
            + cache_gates[:, None, :]
        )
        piece_scores = (
            jnp.einsum(
                "qhd,khd->hqk", query_block, piece_key_heads, preferred_element_type=jnp.float32
            )
            * score_scale
            + piece_bias[:, None, :]
        )
        query_order = first_row + jnp.arange(block_rows, dtype=jnp.int32)
        visible = key_order[None, :] <= query_order[:, None]
        piece_scores = jnp.where(visible[None], piece_scores, -jnp.inf)
        local_max = jnp.maximum(jnp.max(cache_scores, axis=-1), jnp.max(piece_scores, axis=-1))
        cache_exp = jnp.exp(cache_scores - local_max[:, :, None])
        piece_exp = jnp.exp(piece_scores - local_max[:, :, None])
        numerator = jnp.einsum(
            "hqk,khd->qhd",
            cache_exp.astype(jnp.bfloat16),
            cache_value_heads,
            preferred_element_type=jnp.float32,
        )
        numerator = numerator + jnp.einsum(
            "hqk,khd->qhd",
            piece_exp.astype(jnp.bfloat16),
            piece_value_heads,
            preferred_element_type=jnp.float32,
        )
        denominator = jnp.sum(cache_exp, axis=-1) + jnp.sum(piece_exp, axis=-1)
        return (numerator.astype(jnp.bfloat16), denominator.T, local_max.T)

    numerators, denominators, local_maxima = lax.map(block_terms, (query_blocks, block_starts))
    numerators = numerators.reshape(total_rows, local_heads, head_size)
    denominators = denominators.reshape(total_rows, local_heads)
    local_maxima = local_maxima.reshape(total_rows, local_heads)
    maxima = lax.pmax(local_maxima, "kv")
    factors = jnp.exp(local_maxima - maxima)
    scaled = (numerators.astype(jnp.float32) * factors[:, :, None]).astype(jnp.bfloat16)
    rounded = (
        lax.optimization_barrier(scaled)
        .astype(jnp.float32)
        .reshape(total_rows, local_heads * head_size)
    )
    denominators = denominators * factors
    summed = lax.psum(rounded.astype(jnp.bfloat16), "kv").astype(jnp.float32)
    summed_denom = lax.psum(denominators, "kv")
    own_numer = lax.dynamic_slice_in_dim(summed, shard_index * piece_count, piece_count, 0)
    own_denom = lax.dynamic_slice_in_dim(summed_denom, shard_index * piece_count, piece_count, 0)
    piece_attention = (
        own_numer.reshape(piece_count, local_heads, head_size) / own_denom[:, :, None]
    ).astype(jnp.bfloat16)
    piece_attention = piece_attention.reshape(piece_count, local_heads * head_size)
    dec_count = dec_tokens.shape[0]
    dec_span = dec_keys.shape[1]
    dec_query_heads = dec_queries.reshape(dec_count, local_heads, head_size)
    new_key_heads = dec_new_keys.reshape(dec_count, local_heads, head_size)
    new_value_heads = dec_new_values.reshape(dec_count, local_heads, head_size)
    dec_key_heads = dec_keys.reshape(dec_count, dec_span, local_heads, head_size)
    dec_value_heads = dec_values.reshape(dec_count, dec_span, local_heads, head_size)
    cached = (
        jnp.einsum(
            "bhd,bkhd->bhk", dec_query_heads, dec_key_heads, preferred_element_type=jnp.float32
        )
        * score_scale
    )
    cached = cached + dec_gates + dec_gate_now[:, :, None]
    live_slots = jnp.arange(dec_span, dtype=jnp.int32)[None, :] < dec_lengths[:, None]
    cached = jnp.where(live_slots[:, None, :], cached, -jnp.inf)
    own_score = (
        jnp.sum(dec_query_heads.astype(jnp.float32) * new_key_heads.astype(jnp.float32), axis=-1)
        * score_scale
    )
    row_top = jnp.maximum(jnp.max(cached, axis=-1), own_score)
    cached_exp = jnp.exp(cached - row_top[:, :, None])
    own_exp = jnp.exp(own_score - row_top)
    whole_sum = jnp.sum(cached_exp, axis=-1) + own_exp
    cached_weights = (cached_exp / whole_sum[:, :, None]).astype(jnp.bfloat16)
    own_weights = (own_exp / whole_sum).astype(jnp.bfloat16)
    dec_mixed = jnp.einsum(
        "bhk,bkhd->bhd", cached_weights, dec_value_heads, preferred_element_type=jnp.float32
    )
    dec_mixed = dec_mixed + own_weights.astype(jnp.float32)[:, :, None] * new_value_heads.astype(
        jnp.float32
    )
    dec_attention = dec_mixed.astype(jnp.bfloat16).reshape(dec_count, local_heads * head_size)

    def add_columns(columns_in):
        return jnp.dot(columns_in, out_weight, preferred_element_type=jnp.float32)

    piece_out = add_columns(lax.all_gather(piece_attention, "tp", axis=1, tiled=True))
    dec_out = add_columns(lax.all_gather(dec_attention, "tp", axis=1, tiled=True))
    return (piece_out.astype(jnp.bfloat16), dec_out.astype(jnp.bfloat16), piece_keys, piece_values)


def solution(mesh):
    return jax.shard_map(
        shards,
        mesh=mesh,
        in_specs=(
            P(("grp", "kv"), None),
            P(("grp", "kv"), None),
            P(),
            P(None, "tp"),
            P(None, "tp"),
            P(None, "tp"),
            P(None, "tp"),
            P("tp"),
            P(None, "tp"),
            P(("grp", "kv"), "tp"),
            P(("grp", "kv"), "tp"),
            P("tp", ("grp", "kv")),
            P(("grp", "kv"), None, "tp"),
            P(("grp", "kv"), None, "tp"),
            P(("grp", "kv"), "tp", None),
            P(("grp", "kv")),
        ),
        out_specs=(
            P(("grp", "kv"), "tp"),
            P(("grp", "kv"), "tp"),
            P(("grp", "kv"), "tp"),
            P(("grp", "kv"), "tp"),
        ),
        check_vma=False,
    )
```

profile of v0, /device:TPU:0, one launch (start us, length us, event | category | flops | bytes accessed | tf_op | source)
XLA Modules:
  0.0 172.7 jit_solution(16540256553763138558)
XLA Ops:
  7.3 1.6 fusion.21
  9.0 1.8 %fusion.41 = f32[2,256]{1,0:T(2,128)S(1)} fusion(bf16[2048,2]{0,1:T(2,128)(2,1)} %param.26, f32[2]{0:T(128)} %param.27, bf16[256,2048]{1,0:T(8,128)(2,1)} %param.20, f32[2048]{0:T(1024)} %param.22, f32[256]{0:T(256)S(1)} %add_rsqrt_fusion), kind=kOutput, calls=%fused_computation.76 | convolution fusion | flops 4198912 | bytes 1068040 | tf_op jit(solution)/shard_map/dot_general | solution.py:36
  10.8 0.6 reduce-window.6
  11.4 0.2 slice_reduce_fusion
  11.6 0.2 reduce-window.9
  11.8 0.2 slice_reduce_fusion.1
  12.0 12.6 %all-gather = f32[4,1,2]{2,1,0:T(1,128)S(1)} all-gather(f32[1,1,2]{2,1,0:T(1,128)S(1)} %bitcast.143), channel_id=1, replica_groups=mesh['grp'=2,'kv'=4,'tp'=4] {'kv'}, dimensions={0}, use_global_device_ids=true | all-gather | bytes 40 | tf_op jit(solution)/shard_map/all_gather | solution.py:13
  24.7 2.2 %convolution_convert_fusion.2 = bf16[256,256]{0,1:T(8,128)(2,1)S(1)} fusion(bf16[2048,256]{1,0:T(8,128)(2,1)} %param.24, bf16[256,2048]{1,0:T(8,128)(2,1)} %param.20, f32[2048]{0:T(1024)} %param.22, f32[256]{0:T(256)S(1)} %add_rsqrt_fusion), kind=kOutput, calls=%fused_computation.38 | convolution fusion | flops 270598144 | bytes 2237440 | tf_op jit(solution)/shard_map/dot_general | solution.py:31
  26.9 0.8 copy.66
  27.7 2.5 %convolution_convert_fusion.1 = bf16[256,256]{0,1:T(8,128)(2,1)} fusion(bf16[2048,256]{1,0:T(8,128)(2,1)} %param.25, bf16[256,2048]{1,0:T(8,128)(2,1)S(1)} %copy-done.4, f32[2048]{0:T(1024)S(1)} %copy-done.12, f32[256]{0:T(256)S(1)} %add_rsqrt_fusion), kind=kOutput, calls=%fused_computation.37 | convolution fusion | flops 270598144 | bytes 2237440 | tf_op jit(solution)/shard_map/dot_general | solution.py:32
  30.3 1.0 copy.68
  31.3 0.5 convolution_convert_fusion.3
  31.8 14.8 %all_gather.12 = bf16[1024,256]{1,0:T(8,128)(2,1)S(1)} all-gather(bf16[256,256]{1,0:T(8,128)(2,1)S(1)} %convolution_convert_fusion.3), channel_id=1, replica_groups=mesh['grp'=2,'kv'=4,'tp'=4] {'kv'}, dimensions={0}, use_global_device_ids=true | all-gather | bytes 655360 | tf_op jit(solution)/shard_map/all_gather | solution.py:78
  46.6 0.9 reshape.167
  47.5 4.1 %copy.60 = bf16[4096,256]{0,1:T(8,128)(2,1)} copy(bf16[4096,256]{1,0:T(8,128)(2,1)} %param.29) | data formatting | bytes 4194304 | tf_op args[9]
  51.6 3.1 %copy.65 = bf16[4096,2,128]{2,0,1:T(8,128)(2,1)S(1)} copy(bf16[4096,2,128]{0,2,1:T(8,128)(2,1)} %bitcast.130) | data formatting | bytes 4194304
  54.8 4.1 %copy.63 = bf16[4096,256]{0,1:T(8,128)(2,1)} copy(bf16[4096,256]{1,0:T(8,128)(2,1)} %param.30) | data formatting | bytes 4194304 | tf_op args[10]
  58.9 4.1 %copy.67 = bf16[4096,2,128]{2,0,1:T(8,128)(2,1)} copy(bf16[4096,2,128]{0,2,1:T(8,128)(2,1)} %bitcast.131) | data formatting | bytes 4194304
  63.0 43.5 %while.26 = (s32[]{:T(128)}, bf16[2,512,2,128]{3,1,0,2:T(8,128)(2,1)}, f32[2,512,2]{1,2,0:T(2,128)S(1)}, f32[2,512,2]{1,2,0:T(2,128)S(1)}, bf16[2,512,2,128]{3,2...) while((s32[]{:T(128)}, ...), condition=%wide.region_10.11_spmd.clone, body=%wide.region_5.10_spmd.clone.sunk | while | flops 2330327808 | bytes 140415232 | solution.py:129
  63.0 1.1 constant_dynamic-slice_fusion.3
  64.2 0.6 dynamic_slice.32
  64.7 0.6 iota_add_fusion.4
  65.4 0.1 broadcast_compare_fusion.2
  65.6 1.3 fusion.97
  66.9 2.7 %fusion.96 = (f32[2,512]{1,0:T(2,128)S(1)}, f32[2,512,4096]{2,1,0:T(8,128)S(1)}) fusion(f32[2,4096]{1,0:T(2,128)S(1)} %get-tuple-element.431, bf16[4096,2,128]{2,0,1:T(8,128)(2,1)S(1)} %get-tuple-element.430, bf16[1,512,2,128]{3,2,1,0:T(2,128)(2,1)S(1)} %constant_dynamic-slice_fusion.3), kind=kOutput, calls=%fused_computation.4.clone.1 | convolution fusion | flops 1086323712 | bytes 19173376 | tf_op jit(solution)/shard_map/while/body/eval_jaxpr/qhd,khd->hqk/dot_general | solution.py:95
  69.6 0.2 fusion.101
  69.8 3.9 %fusion.100 = f32[2,512]{1,0:T(2,128)S(1)} fusion(f32[2,512,4096]{2,1,0:T(8,128)S(1)} %get-tuple-element.370, f32[2,512]{1,0:T(2,128)S(1)} %get-tuple-element.373, f32[2,4096]{1,0:T(2,128)S(1)} %get-tuple-element.431), kind=kLoop, calls=%fused_computation.5.clone.1 | loop fusion | flops 16776192 | bytes 16818176 | tf_op jit(solution)/shard_map/while/body/eval_jaxpr/reduce_sum | solution.py:126
  73.6 2.3 %copy-done.1 = f32[2,512,4096]{2,1,0:T(8,128)} copy-done((f32[2,512,4096]{2,1,0:T(8,128)}, f32[2,512,4096]{2,1,0:T(8,128)S(1)}, u32[]{:S(2)}) %copy-start.1) | copy-done | bytes 16777240 | tf_op jit(solution)/shard_map/while
  75.9 7.6 %fusion.98 = f32[2,512,128]{2,1,0:T(8,128)S(1)} fusion(bf16[4096,2,128]{2,0,1:T(8,128)(2,1)S(1)} %copy-done.3, f32[2,512,4096]{2,1,0:T(8,128)} %copy-done.1, f32[2,512]{1,0:T(2,128)S(1)} %get-tuple-element.373, f32[2,4096]{1,0:T(2,128)S(1)} %get-tuple-element.431), kind=kOutput, calls=%fused_computation.7.clone.1 | convolution fusion | flops 1090519040 | bytes 19435520 | tf_op jit(solution)/shard_map/while/body/eval_jaxpr/hqk,khd->qhd/dot_general | solution.py:114
  83.5 0.4 fusion.99
  83.9 0.8 copy-done.8
  84.8 1.1 constant_dynamic-slice_fusion.3
  85.9 0.6 dynamic_slice.32
  86.5 0.6 iota_add_fusion.4
  87.1 0.1 broadcast_compare_fusion.2
  87.3 1.3 fusion.97
  88.6 2.7 %fusion.96 = (f32[2,512]{1,0:T(2,128)S(1)}, f32[2,512,4096]{2,1,0:T(8,128)S(1)}) fusion(f32[2,4096]{1,0:T(2,128)S(1)} %get-tuple-element.431, bf16[4096,2,128]{2,0,1:T(8,128)(2,1)S(1)} %get-tuple-element.430, bf16[1,512,2,128]{3,2,1,0:T(2,128)(2,1)S(1)} %constant_dynamic-slice_fusion.3), kind=kOutput, calls=%fused_computation.4.clone.1 | convolution fusion | flops 1086323712 | bytes 19173376 | tf_op jit(solution)/shard_map/while/body/eval_jaxpr/qhd,khd->hqk/dot_general | solution.py:95
  91.3 0.2 fusion.101
  91.5 3.9 %fusion.100 = f32[2,512]{1,0:T(2,128)S(1)} fusion(f32[2,512,4096]{2,1,0:T(8,128)S(1)} %get-tuple-element.370, f32[2,512]{1,0:T(2,128)S(1)} %get-tuple-element.373, f32[2,4096]{1,0:T(2,128)S(1)} %get-tuple-element.431), kind=kLoop, calls=%fused_computation.5.clone.1 | loop fusion | flops 16776192 | bytes 16818176 | tf_op jit(solution)/shard_map/while/body/eval_jaxpr/reduce_sum | solution.py:126
  95.4 2.3 %copy-done.1 = f32[2,512,4096]{2,1,0:T(8,128)} copy-done((f32[2,512,4096]{2,1,0:T(8,128)}, f32[2,512,4096]{2,1,0:T(8,128)S(1)}, u32[]{:S(2)}) %copy-start.1) | copy-done | bytes 16777240 | tf_op jit(solution)/shard_map/while
  97.6 7.6 %fusion.98 = f32[2,512,128]{2,1,0:T(8,128)S(1)} fusion(bf16[4096,2,128]{2,0,1:T(8,128)(2,1)S(1)} %copy-done.3, f32[2,512,4096]{2,1,0:T(8,128)} %copy-done.1, f32[2,512]{1,0:T(2,128)S(1)} %get-tuple-element.373, f32[2,4096]{1,0:T(2,128)S(1)} %get-tuple-element.431), kind=kOutput, calls=%fused_computation.7.clone.1 | convolution fusion | flops 1090519040 | bytes 19435520 | tf_op jit(solution)/shard_map/while/body/eval_jaxpr/hqk,khd->qhd/dot_general | solution.py:114
  105.2 0.4 fusion.99
  105.7 0.8 copy-done.8
  106.5 9.4 %pmax.7 = f32[1024,2]{0,1:T(2,128)S(1)} all-reduce(f32[1024,2]{0,1:T(2,128)S(1)} %bitcast.135), channel_id=1, replica_groups=mesh['grp'=2,'kv'=4,'tp'=4] {'kv'}, use_global_device_ids=true, to_apply=%region_11.12 | all-reduce | flops 2048 | bytes 16384 | tf_op jit(solution)/shard_map/pmax | solution.py:133
  115.9 1.4 fusion.29
  117.3 1.0 copy.70
  118.6 1.5 convolution_convert_fusion.7
  120.2 1.5 fusion.25
  121.7 0.3 fusion.24
  121.9 0.8 copy.72
  122.7 0.8 copy.73
  123.5 6.3 %copy.82 = bf16[4,2048,256]{1,2,0:T(8,128)(2,1)} copy(bf16[4,2048,256]{2,1,0:T(8,128)(2,1)} %param.32) | data formatting | bytes 8388608 | tf_op jit(solution)/shard_map/reshape | solution.py:155
  130.0 2.8 %fusion.54 = f32[4,2,1,2048]{3,2,1,0:T(1,128)S(1)} fusion(bf16[4,2,128,1]{2,3,1,0:T(2,128)(2,1)S(1)} %reshape.190, bf16[4,2048,2,128]{1,3,2,0:T(8,128)(2,1)} %bitcast.129), kind=kOutput, calls=%fused_computation.97 | convolution fusion | flops 4194304 | bytes 4261888 | tf_op jit(solution)/shard_map/bhd,bkhd->bhk/dot_general | solution.py:158
  132.9 0.2 fusion.50
  133.1 0.2 fusion.35
  133.3 0.1 fusion.39
  133.5 2.9 %fusion.18 = f32[4,2,1,128]{3,2,1,0:T(1,128)S(1)} fusion(bf16[4,2,2048,1]{2,1,0,3:T(2,128)(2,1)S(1)} %fusion.39, bf16[4,2048,256]{2,1,0:T(8,128)(2,1)} %param.33), kind=kOutput, calls=%fused_computation.28 | convolution fusion | flops 4194304 | bytes 4231168 | tf_op jit(solution)/shard_map/bhk,bkhd->bhd/dot_general | solution.py:176
  136.4 5.2 %all_gather.15 = bf16[4,1024]{1,0:T(4,128)(2,1)S(1)} all-gather(bf16[4,256]{1,0:T(4,128)(2,1)S(1)} %bitcast.139), channel_id=1, replica_groups=mesh['grp'=2,'kv'=4,'tp'=4] {'tp'}, dimensions={1}, use_global_device_ids=true | all-gather | bytes 10240 | tf_op jit(solution)/shard_map/all_gather | solution.py:188
  141.6 10.5 %psum.15 = f32[1024,2]{0,1:T(2,128)S(1)} all-reduce(f32[1024,2]{0,1:T(2,128)S(1)} %get-tuple-element.251), channel_id=1, replica_groups=mesh['grp'=2,'kv'=4,'tp'=4] {'kv'}, use_global_device_ids=true, to_apply=%region_13.14 | all-reduce | flops 2048 | bytes 16384 | tf_op jit(solution)/shard_map/psum | solution.py:143
  152.1 0.8 convolution_convert_fusion.4
  153.0 3.7 %all-reduce.2.cloned.1.call-done = bf16[1024,256]{0,1:T(8,128)(2,1)} async-done(((bf16[1024,256]{0,1:T(8,128)(2,1)}), bf16[1024,256]{0,1:T(8,128)(2,1)}) %all-reduce.2.cloned.1.call-update) | async-done | bytes 524304 | tf_op jit(solution)/shard_map/psum | solution.py:142
  156.7 0.9 fusion.30
  157.6 7.1 %all_gather.14 = bf16[256,1024]{0,1:T(8,128)(2,1)S(1)} all-gather(bf16[256,256]{0,1:T(8,128)(2,1)S(1)} %fusion.30), channel_id=1, replica_groups=mesh['grp'=2,'kv'=4,'tp'=4] {'tp'}, dimensions={1}, use_global_device_ids=true | all-gather | bytes 655360 | tf_op jit(solution)/shard_map/all_gather | solution.py:187
  164.7 1.2 convolution_convert_fusion
  (72 shorter events, 1.2 us)
Async XLA Ops:
  7.2 145.0 %copy-start = (bf16[1024,512]{1,0:T(8,128)(2,1)S(1)}, bf16[1024,512]{1,0:T(8,128)(2,1)}, u32[]{:S(2)}) copy-start(bf16[1024,512]{1,0:T(8,128)(2,1)} %param.28) | copy-start | bytes 3145732
  7.2 20.5 %copy-start.4 = (bf16[256,2048]{1,0:T(8,128)(2,1)S(1)}, bf16[256,2048]{1,0:T(8,128)(2,1)}, u32[]{:S(2)}) copy-start(bf16[256,2048]{1,0:T(8,128)(2,1)} %param.20) | copy-start | bytes 3145732
  7.2 20.5 %copy-start.12 = (f32[2048]{0:T(1024)S(1)}, f32[2048]{0:T(1024)}, u32[]{:S(2)}) copy-start(f32[2048]{0:T(1024)} %param.22) | copy-start | bytes 24580
  7.2 149.5 %all-reduce.2.cloned.1.call-start = ((), (), s32[]{:S(2)}) async-start(), calls=%async_computation | async-start | bytes 1048576 | tf_op jit(solution)/shard_map/psum | solution.py:142
  8.9 22.3 %copy-start.5 = (bf16[2048,256]{1,0:T(8,128)(2,1)S(1)}, bf16[2048,256]{1,0:T(8,128)(2,1)}, u32[]{:S(2)}) copy-start(bf16[2048,256]{1,0:T(8,128)(2,1)} %param.23) | copy-start | bytes 3145732
  54.7 8.2 %copy-start.2 = (f32[2,4096]{1,0:T(2,128)S(1)}, f32[2,4096]{1,0:T(2,128)}, u32[]{:S(2)}) copy-start(f32[2,4096]{1,0:T(2,128)} %param.31) | copy-start | bytes 98308
  63.0 55.4 %copy-start.11 = (bf16[4,2048]{1,0:T(4,128)(2,1)S(1)}, bf16[4,2048]{1,0:T(4,128)(2,1)}, u32[]{:S(2)}) copy-start(bf16[4,2048]{1,0:T(4,128)(2,1)} %param.21) | copy-start | bytes 49156
  63.0 57.1 %copy-start.14 = (bf16[2048,2]{0,1:T(2,128)(2,1)S(1)}, bf16[2048,2]{0,1:T(2,128)(2,1)}, u32[]{:S(2)}) copy-start(bf16[2048,2]{0,1:T(2,128)(2,1)} %param.26) | copy-start | bytes 24580
  63.0 57.1 %copy-start.15 = (f32[2]{0:T(128)S(1)}, f32[2]{0:T(128)}, u32[]{:S(2)}) copy-start(f32[2]{0:T(128)} %param.27) | copy-start | bytes 28
  69.6 6.3 %copy-start.1 = (f32[2,512,4096]{2,1,0:T(8,128)}, f32[2,512,4096]{2,1,0:T(8,128)S(1)}, u32[]{:S(2)}) copy-start(f32[2,512,4096]{2,1,0:T(8,128)S(1)} %get-tuple-element.370) | copy-start | bytes 50331652 | tf_op jit(solution)/shard_map/while
  69.8 6.1 %copy-start.3 = (bf16[4096,2,128]{2,0,1:T(8,128)(2,1)S(1)}, bf16[4096,2,128]{2,0,1:T(8,128)(2,1)}, u32[]{:S(2)}) copy-start(bf16[4096,2,128]{2,0,1:T(8,128)(2,1)} %get-tuple-element.435) | copy-start | bytes 6291460 | tf_op jit(solution)/shard_map/while
  75.9 7.6 %copy-start.7 = (bf16[2,512,2,128]{3,1,0,2:T(8,128)(2,1)S(1)}, bf16[2,512,2,128]{3,1,0,2:T(8,128)(2,1)}, u32[]{:S(2)}) copy-start(bf16[2,512,2,128]{3,1,0,2:T(8,128)(2,1)} %get-tuple-element.412) | copy-start | bytes 1572868 | tf_op jit(solution)/shard_map/while
  83.9 0.8 copy-start.8
  91.3 6.3 %copy-start.1 = (f32[2,512,4096]{2,1,0:T(8,128)}, f32[2,512,4096]{2,1,0:T(8,128)S(1)}, u32[]{:S(2)}) copy-start(f32[2,512,4096]{2,1,0:T(8,128)S(1)} %get-tuple-element.370) | copy-start | bytes 50331652 | tf_op jit(solution)/shard_map/while
  91.5 6.1 %copy-start.3 = (bf16[4096,2,128]{2,0,1:T(8,128)(2,1)S(1)}, bf16[4096,2,128]{2,0,1:T(8,128)(2,1)}, u32[]{:S(2)}) copy-start(bf16[4096,2,128]{2,0,1:T(8,128)(2,1)} %get-tuple-element.435) | copy-start | bytes 6291460 | tf_op jit(solution)/shard_map/while
  97.6 7.6 %copy-start.7 = (bf16[2,512,2,128]{3,1,0,2:T(8,128)(2,1)S(1)}, bf16[2,512,2,128]{3,1,0,2:T(8,128)(2,1)}, u32[]{:S(2)}) copy-start(bf16[2,512,2,128]{3,1,0,2:T(8,128)(2,1)} %get-tuple-element.412) | copy-start | bytes 1572868 | tf_op jit(solution)/shard_map/while
  105.7 0.8 copy-start.8
  106.5 15.2 %copy-start.6 = (bf16[2048,256]{1,0:T(8,128)(2,1)S(1)}, bf16[2048,256]{1,0:T(8,128)(2,1)}, u32[]{:S(2)}) copy-start(bf16[2048,256]{1,0:T(8,128)(2,1)} %param.25) | copy-start | bytes 3145732
  106.5 16.2 %copy-start.9 = (bf16[256,256]{0,1:T(8,128)(2,1)S(1)}, bf16[256,256]{0,1:T(8,128)(2,1)}, u32[]{:S(2)}) copy-start(bf16[256,256]{0,1:T(8,128)(2,1)} %convolution_convert_fusion.1) | copy-start | bytes 393220
  123.5 6.4 %copy-start.13 = (s32[4]{0:T(128)S(1)}, s32[4]{0:T(128)}, u32[]{:S(2)}) copy-start(s32[4]{0:T(128)} %param.35) | copy-start | bytes 52
  129.8 3.1 %copy-start.10 = (f32[4,2,2048]{2,1,0:T(2,128)S(1)}, f32[4,2,2048]{2,1,0:T(2,128)}, u32[]{:S(2)}) copy-start(f32[4,2,2048]{2,1,0:T(2,128)} %param.34) | copy-start | bytes 196612
Sparse Core Ops, SparseCore 0:
  118.5 38.1 all-reduce.1
where the time goes:
time: 174 us; the launch traced here: 173 us
  blocking collectives  59.6 us (34%)
  matrix products  42.1 us (24%)
  local copies, waits for them, and re-layouts  37.2 us (21%)
  other arithmetic  15.6 us (9%)
  between operations  14.3 us (8%)
  waiting for transfers between devices  3.7 us (2%)
    unnamed x34, local copies, waits for them, and re-layouts  18.9 us
    dot_general x2, matrix products, block_terms(): jnp.einsum('hqk,khd->qhd', cache_exp.astype(jnp.bfloat16), cache_value_he...  15.1 us
    all_gather x1, blocking collectives, shards(): all_queries = lax.all_gather(piece_queries, 'kv', axis=0, tiled=True)  14.8 us
    all_gather x1, blocking collectives, carried_in(): gathered = lax.all_gather(part, axis)  12.6 us
    psum x1, blocking collectives, shards(): summed_denom = lax.psum(denominators, 'kv')  10.5 us
    pmax x1, blocking collectives, shards(): maxima = lax.pmax(local_maxima, 'kv')  9.36 us
    reduce_sum x4, other arithmetic, block_terms(): denominator = jnp.sum(cache_exp, axis=-1) + jnp.sum(piece_exp, axis=-1)  8.03 us
    all_gather x1, blocking collectives, shards(): lax.all_gather(piece_attention, 'tp', axis=1, tiled=True)  7.13 us
  transfers between devices with their start and end apart: 1, of which 1 were waited for; matrix products, arithmetic and copies ran while one was open for 11% of the time, Pallas kernels for 0%

commit v1 on v0

v1 whole, which is shorter than its diff:
```python
import functools
import math

import jax
import jax.numpy as jnp
from jax import lax
from jax.experimental import pallas as pl
from jax.experimental.pallas import tpu as pltpu
from jax.sharding import PartitionSpec as P

norm_eps = 1e-05
LOG2E = math.log2(math.e)
MESH = pl.DeviceIdType.MESH
NT = (((1,), (1,)), ((), ()))
F32 = jnp.float32
BF16 = jnp.bfloat16


def xor(a, k, n):
    out, bit = 0, 1
    while bit < n:
        out = out + ((a // bit + k // bit) % 2) * bit
        bit *= 2
    return out


def rms(values, gain):
    factor = lax.rsqrt(jnp.mean(values * values, axis=-1, keepdims=True) + norm_eps)
    return values * factor * gain


def lane_fold(op, values):
    out = values[:, :128]
    for i in range(1, values.shape[1] // 128):
        out = op(out, values[:, i * 128 : (i + 1) * 128])
    return out


def kernel(
    n, t, heads,
    piece_x, dec_x, gain, qw, kw, vw, fwt, fb, ow, ck, cv, cg, dk, dv, dg, dl,
    out_p, out_d, out_k, out_v,
    xs, qws, kws, vws, ows, cks, cvs, dks, dvs,
    normed, qall, tots, numsend, numrecv, statsend, statrecv, attn_own, attn_recv,
    kbuf, vbuf, cgs, dgs, pbias, sbuf,
    load_sem, store_sem, q_ssem, q_rsem, t_ssem, t_rsem, n_ssem, n_rsem, s_ssem, s_rsem, a_ssem, a_rsem,
):
    me = lax.axis_index("kv")
    tp = lax.axis_index("tp")
    rows = xs.shape[0]
    all_rows = normed.shape[0]
    width = qws.shape[1]
    hd = width // heads
    dec = dec_x.shape[0]
    cache_rows = cks.shape[0]
    span = dks.shape[1]
    scale = hd ** (-0.5)
    scale2 = scale * LOG2E

    loads = [
        pltpu.make_async_copy(src, dst, load_sem.at[i])
        for i, (src, dst) in enumerate(
            [(piece_x, xs), (qw, qws), (kw, kws), (vw, vws), (dk, dks), (dv, dvs), (ck, cks), (cv, cvs), (ow, ows)]
        )
    ]
    for i in range(4):
        loads[i].start()

    barrier = pltpu.get_barrier_semaphore()
    for k in range(1, n):
        pl.semaphore_signal(barrier, inc=1, device_id={"kv": xor(me, k, n)}, device_id_type=MESH)
    for k in range(1, t):
        pl.semaphore_signal(barrier, inc=1, device_id={"tp": lax.rem(tp + k, t)}, device_id_type=MESH)

    g = gain[...]
    dec_normed = rms(dec_x[...].astype(F32), g)
    pad = all_rows - rows - dec
    normed[rows:, :] = jnp.concatenate([dec_normed, jnp.zeros((pad, g.shape[1]), F32)], 0).astype(BF16)
    loads[0].wait()
    step = 64
    for i in range(0, rows, step):
        normed[i : i + step, :] = rms(xs[i : i + step, :].astype(F32), g).astype(BF16)
    for i in range(4, 9):
        loads[i].start()
    loads[1].wait()
    q = jnp.dot(normed[...], qws[...], preferred_element_type=F32).astype(BF16)
    qall[0] = q[:rows]
    dec_q = q[rows:].astype(F32)
    pl.semaphore_wait(barrier, n - 1 + t - 1)

    def q_copy(k):
        return pltpu.make_async_remote_copy(
            src_ref=qall.at[0], dst_ref=qall.at[k], send_sem=q_ssem.at[k], recv_sem=q_rsem.at[k],
            device_id={"kv": xor(me, k, n)}, device_id_type=MESH)

    def t_copy(k):
        return pltpu.make_async_remote_copy(
            src_ref=tots.at[0], dst_ref=tots.at[k], send_sem=t_ssem.at[k], recv_sem=t_rsem.at[k],
            device_id={"kv": xor(me, k, n)}, device_id_type=MESH)

    def n_copy(k):
        return pltpu.make_async_remote_copy(
            src_ref=numsend.at[k], dst_ref=numrecv.at[k], send_sem=n_ssem.at[k], recv_sem=n_rsem.at[k],
            device_id={"kv": xor(me, k, n)}, device_id_type=MESH)

    def s_copy(k):
        return pltpu.make_async_remote_copy(
            src_ref=statsend.at[k], dst_ref=statrecv.at[k], send_sem=s_ssem.at[k], recv_sem=s_rsem.at[k],
            device_id={"kv": xor(me, k, n)}, device_id_type=MESH)

    for k in range(1, n):
        q_copy(k).start()

    z = lax.dot_general(fwt[...], normed[...], NT, preferred_element_type=F32) + fb[...]
    log_gates = jnp.minimum(z, 0.0) - jnp.log1p(jnp.exp(-jnp.abs(z)))
    earlier = lax.broadcasted_iota(jnp.int32, (rows, rows), 0) <= lax.broadcasted_iota(jnp.int32, (rows, rows), 1)
    running = lax.dot_general(
        log_gates[:, :rows], earlier.astype(F32), (((1,), (0,)), ((), ())),
        precision=lax.Precision.HIGHEST, preferred_element_type=F32)
    tots[0] = jnp.zeros((8, 128), F32)
    tots[0, :heads, :] = jnp.broadcast_to(running[:, rows - 1 :], (heads, 128))
    for k in range(1, n):
        t_copy(k).start()

    loads[2].wait()
    keys = jnp.dot(normed[...], kws[...], preferred_element_type=F32).astype(BF16)
    kbuf[...] = keys[:rows]
    dec_k = keys[rows:].astype(F32)
    loads[3].wait()
    values = jnp.dot(normed[...], vws[...], preferred_element_type=F32).astype(BF16)
    vbuf[...] = values[:rows]
    dec_v = values[rows:].astype(F32)
    stores = [pltpu.make_async_copy(kbuf, out_k, store_sem.at[0]), pltpu.make_async_copy(vbuf, out_v, store_sem.at[1])]
    for copy in stores:
        copy.start()

    cgs[...] = cg[...] * LOG2E

    drows = dgs.shape[0]
    row_w = lax.broadcasted_iota(jnp.int32, (drows, width), 0)
    lane_w = lax.broadcasted_iota(jnp.int32, (drows, width), 1)
    masks = [(row_w == b * heads + lane_w // hd) for b in range(dec)]
    row_1 = lax.broadcasted_iota(jnp.int32, (drows, 1), 0)
    if drows > dec * heads:
        dgs[...] = jnp.zeros(dgs.shape, F32)
    own_score = jnp.zeros((drows, 1), F32)
    live = jnp.ones((drows, 1), jnp.int32)
    now = jnp.zeros((drows, 1), F32)
    loads[4].wait()
    scores = jnp.zeros((drows, span), F32)
    for b in range(dec):
        dgs[b * heads : (b + 1) * heads, :] = dg[b]
        qb = jnp.where(masks[b], jnp.broadcast_to(dec_q[b : b + 1], (drows, width)), 0.0)
        own_score = own_score + jnp.sum(qb * dec_k[b : b + 1], axis=1, keepdims=True)
        live = jnp.where(row_1 // heads == b, dl[b], live)
        for h in range(heads):
            now = jnp.where(row_1 == b * heads + h, log_gates[h : h + 1, rows + b : rows + b + 1], now)
        scores = scores + lax.dot_general(qb.astype(BF16), dks[b], NT, preferred_element_type=F32)
    scores = scores * scale2 + (dgs[...] + now) * LOG2E
    scores = jnp.where(lax.broadcasted_iota(jnp.int32, (drows, span), 1) < live, scores, -jnp.inf)
    own_score = own_score * scale2
    top = jnp.maximum(jnp.max(scores, axis=1, keepdims=True), own_score)
    e = jnp.exp2(scores - top)
    own_e = jnp.exp2(own_score - top)
    whole = jnp.sum(e, axis=1, keepdims=True) + own_e
    w = (e / whole).astype(BF16)
    own_w = (own_e / whole).astype(BF16).astype(F32)
    loads[5].wait()
    outs = []
    for b in range(dec):
        mixed = jnp.dot(w, dvs[b], preferred_element_type=F32) + own_w * dec_v[b : b + 1]
        outs.append(jnp.sum(jnp.where(masks[b], mixed, 0.0), axis=0, keepdims=True))
    outs.append(jnp.zeros((pad, width), F32))
    attn_own[rows:, :] = jnp.concatenate(outs, 0).astype(BF16)

    offset = jnp.zeros((8, 128), F32)
    for k in range(1, n):
        t_copy(k).wait_recv()
        offset = offset + jnp.where(xor(me, k, n) < me, tots[k], 0.0)
    pbias[...] = -(running + offset[:heads, :1]) * LOG2E

    loads[6].wait()
    loads[7].wait()
    lane_s = lax.broadcasted_iota(jnp.int32, (rows, 128), 1)
    chunk = math.gcd(cache_rows, 1024)

    def attend(lap, carry):
        k = lax.rem(lap, n)

        @pl.when(k != 0)
        def _():
            q_copy(k).wait_recv()

        owner = xor(me, k, n)
        first = owner * rows - me * rows
        stats = jnp.zeros((rows, 128), F32)
        for h in range(heads):
            hs = slice(h * hd, (h + 1) * hd)
            qh = qall[k, :, hs]
            s = lax.dot_general(qh, kbuf[:, hs], NT, preferred_element_type=F32) * scale2 + pbias[h : h + 1, :]
            seen = lax.broadcasted_iota(jnp.int32, (rows, rows), 1) <= lax.broadcasted_iota(jnp.int32, (rows, rows), 0) + first
            s = jnp.where(seen, s, -jnp.inf)
            sbuf[h, :, cache_rows:] = s
            top = lane_fold(jnp.maximum, s)
            for c in range(0, cache_rows, chunk):
                s = lax.dot_general(qh, cks[c : c + chunk, hs], NT, preferred_element_type=F32) * scale2 + cgs[h : h + 1, c : c + chunk]
                sbuf[h, :, c : c + chunk] = s
                top = jnp.maximum(top, lane_fold(jnp.maximum, s))
            m = jnp.max(top, axis=1, keepdims=True)
            p = jnp.exp2(sbuf[h, :, cache_rows:] - m)
            total = lane_fold(jnp.add, p)
            o = jnp.dot(p.astype(BF16), vbuf[:, hs], preferred_element_type=F32)
            for c in range(0, cache_rows, chunk):
                p = jnp.exp2(sbuf[h, :, c : c + chunk] - m)
                total = total + lane_fold(jnp.add, p)
                o = o + jnp.dot(p.astype(BF16), cvs[c : c + chunk, hs], preferred_element_type=F32)
            l = jnp.sum(total, axis=1, keepdims=True)
            numsend[k, :, hs] = o.astype(BF16)
            stats = jnp.where(lane_s == 2 * h, m, jnp.where(lane_s == 2 * h + 1, l, stats))
        statsend[k] = stats.T[: statsend.shape[1]]

        @pl.when(k != 0)
        def _():
            n_copy(k).start()
            s_copy(k).start()

        return carry

    lax.fori_loop(1, n + 1, attend, 0)

    stats = [statsend[0]]
    for k in range(1, n):
        s_copy(k).wait_recv()
        stats.append(statrecv[k])
    weights = []
    for h in range(heads):
        m = stats[0][2 * h : 2 * h + 1]
        for k in range(1, n):
            m = jnp.maximum(m, stats[k][2 * h : 2 * h + 1])
        fs = [jnp.exp2(s[2 * h : 2 * h + 1] - m) for s in stats]
        l = fs[0] * stats[0][2 * h + 1 : 2 * h + 2]
        for k in range(1, n):
            l = l + fs[k] * stats[k][2 * h + 1 : 2 * h + 2]
        weights += [f / l for f in fs]
    weights.append(jnp.zeros((128 - heads * n, rows), F32))
    cols = jnp.concatenate(weights, 0).T
    for k in range(1, n):
        n_copy(k).wait_recv()
    for h in range(heads):
        hs = slice(h * hd, (h + 1) * hd)
        acc = numsend[0, :, hs].astype(F32) * cols[:, h * n : h * n + 1]
        for k in range(1, n):
            acc = acc + numrecv[k, :, hs].astype(F32) * cols[:, h * n + k : h * n + k + 1]
        attn_own[:rows, hs] = acc.astype(BF16)

    mate = tp + 1 - 2 * (tp % 2)

    def a_copy(k):
        return pltpu.make_async_remote_copy(
            src_ref=attn_own, dst_ref=attn_recv.at[k], send_sem=a_ssem.at[k], recv_sem=a_rsem.at[k],
            device_id={"tp": (tp + k) % t}, device_id_type=MESH)

    def b_copy(k):
        return pltpu.make_async_remote_copy(
            src_ref=attn_recv.at[k], dst_ref=attn_recv.at[k + 1], send_sem=a_ssem.at[k + 1], recv_sem=a_rsem.at[k + 1],
            device_id={"tp": mate}, device_id_type=MESH)

    mate_copy = pltpu.make_async_remote_copy(
        src_ref=attn_own, dst_ref=attn_recv.at[1], send_sem=a_ssem.at[1], recv_sem=a_rsem.at[1],
        device_id={"tp": mate}, device_id_type=MESH)
    for k in range(2, t, 2):
        a_copy(k).start()
    mate_copy.start()
    loads[8].wait()

    def part(block, who):
        return jnp.dot(block, ows[pl.ds(pl.multiple_of(who * width, width), width), :], preferred_element_type=F32)

    acc = part(attn_own[...], tp)
    mate_copy.wait_recv()
    acc = acc + part(attn_recv[1], mate)
    for k in range(2, t, 2):
        a_copy(k).wait_recv()
        b_copy(k).start()
        acc = acc + part(attn_recv[k], (tp + t - k) % t)
    for k in range(2, t, 2):
        b_copy(k).wait_recv()
        acc = acc + part(attn_recv[k + 1], (mate + t - k) % t)
    out_p[...] = acc[:rows].astype(BF16)
    out_d[...] = acc[rows : rows + dec].astype(BF16)

    for copy in stores:
        copy.wait()
    for k in range(1, n):
        q_copy(k).wait_send()
        t_copy(k).wait_send()
        n_copy(k).wait_send()
        s_copy(k).wait_send()
    mate_copy.wait_send()
    for k in range(2, t, 2):
        a_copy(k).wait_send()
        b_copy(k).wait_send()


def shards(
    n, t,
    piece_tokens, dec_tokens, norm_gain, query_weight, key_weight, value_weight, forget_weight, forget_bias,
    out_weight, cache_keys, cache_values, cache_gates, dec_keys, dec_values, dec_gates, dec_lengths,
):
    rows, depth = piece_tokens.shape
    heads = forget_weight.shape[1]
    width = query_weight.shape[1]
    dec = dec_tokens.shape[0]
    all_rows = rows + -(-dec // 16) * 16
    cols = out_weight.shape[1]
    cache_rows = cache_keys.shape[0]
    drows = -(-dec * heads // 8) * 8
    stat_rows = -(-2 * heads // 8) * 8
    any_space = pl.BlockSpec(memory_space=pl.ANY)
    vmem = pl.BlockSpec(memory_space=pltpu.VMEM)
    smem = pl.BlockSpec(memory_space=pltpu.SMEM)

    def like(array):
        return pltpu.VMEM(array.shape, array.dtype)

    dma = pltpu.SemaphoreType.DMA
    return pl.pallas_call(
        functools.partial(kernel, n, t, heads),
        out_shape=(
            jax.ShapeDtypeStruct((rows, cols), BF16),
            jax.ShapeDtypeStruct((dec, cols), BF16),
            jax.ShapeDtypeStruct((rows, width), BF16),
            jax.ShapeDtypeStruct((rows, width), BF16),
        ),
        in_specs=[any_space, vmem, vmem, any_space, any_space, any_space, vmem, vmem, any_space,
                  any_space, any_space, vmem, any_space, any_space, vmem, smem],
        out_specs=(vmem, vmem, any_space, any_space),
        scratch_shapes=[
            like(piece_tokens), like(query_weight), like(key_weight), like(value_weight), like(out_weight),
            like(cache_keys), like(cache_values), like(dec_keys), like(dec_values),
            pltpu.VMEM((all_rows, depth), BF16),
            pltpu.VMEM((n, rows, width), BF16),
            pltpu.VMEM((n, 8, 128), F32),
            pltpu.VMEM((n, rows, width), BF16),
            pltpu.VMEM((n, rows, width), BF16),
            pltpu.VMEM((n, stat_rows, rows), F32),
            pltpu.VMEM((n, stat_rows, rows), F32),
            pltpu.VMEM((all_rows, width), BF16),
            pltpu.VMEM((t, all_rows, width), BF16),
            pltpu.VMEM((rows, width), BF16),
            pltpu.VMEM((rows, width), BF16),
            like(cache_gates),
            pltpu.VMEM((drows, dec_keys.shape[1]), F32),
            pltpu.VMEM((heads, rows), F32),
            pltpu.VMEM((heads, rows, cache_rows + rows), F32),
            dma((9,)), dma((2,)),
            dma((n,)), dma((n,)), dma((n,)), dma((n,)), dma((n,)), dma((n,)), dma((n,)), dma((n,)),
            dma((t,)), dma((t,)),
        ],
        compiler_params=pltpu.CompilerParams(
            collective_id=0, has_side_effects=True, vmem_limit_bytes=60 * 1024 * 1024),
    )(
        piece_tokens, dec_tokens, norm_gain.reshape(1, depth), query_weight, key_weight, value_weight,
        forget_weight.T, forget_bias.reshape(heads, 1), out_weight, cache_keys, cache_values, cache_gates,
        dec_keys, dec_values, dec_gates, dec_lengths,
    )


def solution(mesh):
    rows = P(("grp", "kv"), None)
    both = P(("grp", "kv"), "tp")
    cols = P(None, "tp")
    deep = P(("grp", "kv"), None, "tp")
    return jax.shard_map(
        functools.partial(shards, mesh.shape["kv"], mesh.shape["tp"]),
        mesh=mesh,
        in_specs=(
            rows, rows, P(), cols, cols, cols, cols, P("tp"), cols, both, both, P("tp", ("grp", "kv")),
            deep, deep, P(("grp", "kv"), "tp", None), P(("grp", "kv")),
        ),
        out_specs=(both, both, both, both),
        check_vma=False,
    )
```

time: 174 us -> 54.2 us (0.31)
  the two profiles are of different devices: /device:TPU:0 before, /device:TPU:21 now
where the time goes in v1:
time: 54.2 us; the launch traced here: 53.9 us
  Pallas kernels  45.9 us (85%)
  local copies, waits for them, and re-layouts  7.37 us (14%)
  between operations  0.64 us (1%)
    pallas_call x1, Pallas kernels, shards(): pl.pallas_call(functools.partial(kernel, n, t, heads), out_shape=(jax.Sha...  45.9 us
    unnamed x4, local copies, waits for them, and re-layouts  6.07 us
    reshape x1, local copies, waits for them, and re-layouts, shards(): forget_bias.reshape(heads, 1)  1.3 us

profile of v1, /device:TPU:21, one launch (start us, length us, event | category | flops | bytes accessed | tf_op | source)
XLA Modules:
  0.0 53.9 jit_solution(12230649861587858232)
XLA Ops:
  0.6 1.3 %copy.20.fb = f32[2,1]{1,0:T(2,128)} copy(f32[2,1]{0,1:T(1,128)} %bitcast.5) | data formatting | bytes 16 | tf_op jit(solution)/shard_map/reshape | solution.py:364
  1.9 45.9 %shard_map.183 = (bf16[256,512]{1,0:T(8,128)(2,1)}, bf16[4,512]{1,0:T(4,128)(2,1)}, bf16[256,256]{1,0:T(8,128)(2,1)}, bf16[256,256]{1,0:T(8,128)(2,1)}) custom-call(bf16[256,2048]{1,0:T(8,128)(2,1)} %piece_x.1, bf16[4,2048]{1,0:T(4,128)(2,1)} %dec_x.1, f32[1,2048]{1,0:T(1,128)} %bitcast.3, bf16[2048,256]{1,0:T(8,128)(2,1)} %qw.1, bf16[2048,256]{1,0:T(8,128)(2,1)} %kw.1, ...), custom_call_target="tpu_custom_call" | custom-call | tf_op jit(solution)/shard_map/pallas_call | solution.py:327
  47.9 1.7 %copy.25 = bf16[256,512]{1,0:T(8,128)(2,1)} copy(bf16[256,512]{1,0:T(8,128)(2,1)} %get-tuple-element.8) | data formatting | bytes 524288
  49.5 1.3 %copy.26 = bf16[4,512]{1,0:T(4,128)(2,1)} copy(bf16[4,512]{1,0:T(4,128)(2,1)} %get-tuple-element.9) | data formatting | bytes 8192
  50.8 1.6 %copy.27 = bf16[256,256]{1,0:T(8,128)(2,1)} copy(bf16[256,256]{1,0:T(8,128)(2,1)} %get-tuple-element.10) | data formatting | bytes 262144
  52.4 1.6 %copy.28 = bf16[256,256]{1,0:T(8,128)(2,1)} copy(bf16[256,256]{1,0:T(8,128)(2,1)} %get-tuple-element.11) | data formatting | bytes 262144

commit v2 on v1

--- a/solution.py
+++ b/solution.py
@@ -98,9 +98,9 @@
             src_ref=tots.at[0], dst_ref=tots.at[k], send_sem=t_ssem.at[k], recv_sem=t_rsem.at[k],
             device_id={"kv": xor(me, k, n)}, device_id_type=MESH)
 
-    def n_copy(k):
-        return pltpu.make_async_remote_copy(
-            src_ref=numsend.at[k], dst_ref=numrecv.at[k], send_sem=n_ssem.at[k], recv_sem=n_rsem.at[k],
+    def n_copy(k, h):
+        return pltpu.make_async_remote_copy(
+            src_ref=numsend.at[k, h], dst_ref=numrecv.at[k, h], send_sem=n_ssem.at[k, h], recv_sem=n_rsem.at[k, h],
             device_id={"kv": xor(me, k, n)}, device_id_type=MESH)
 
     def s_copy(k):
@@ -108,10 +108,14 @@
             src_ref=statsend.at[k], dst_ref=statrecv.at[k], send_sem=s_ssem.at[k], recv_sem=s_rsem.at[k],
             device_id={"kv": xor(me, k, n)}, device_id_type=MESH)
 
-    for k in range(1, n):
+    for k in range(n - 1, 0, -1):
         q_copy(k).start()
 
-    z = lax.dot_general(fwt[...], normed[...], NT, preferred_element_type=F32) + fb[...]
+    z = lax.dot_general(fwt[...], normed[...], NT, preferred_element_type=F32)
+    bias = jnp.zeros(z.shape, F32)
+    for h in range(heads):
+        bias = jnp.where(lax.broadcasted_iota(jnp.int32, z.shape, 0) == h, fb[h], bias)
+    z = z + bias
     log_gates = jnp.minimum(z, 0.0) - jnp.log1p(jnp.exp(-jnp.abs(z)))
     earlier = lax.broadcasted_iota(jnp.int32, (rows, rows), 0) <= lax.broadcasted_iota(jnp.int32, (rows, rows), 1)
     running = lax.dot_general(
@@ -171,7 +175,9 @@
         mixed = jnp.dot(w, dvs[b], preferred_element_type=F32) + own_w * dec_v[b : b + 1]
         outs.append(jnp.sum(jnp.where(masks[b], mixed, 0.0), axis=0, keepdims=True))
     outs.append(jnp.zeros((pad, width), F32))
-    attn_own[rows:, :] = jnp.concatenate(outs, 0).astype(BF16)
+    dec_attn = jnp.concatenate(outs, 0).astype(BF16)
+    for h in range(heads):
+        attn_own[h, rows:, :] = dec_attn[:, h * hd : (h + 1) * hd]
 
     offset = jnp.zeros((8, 128), F32)
     for k in range(1, n):
@@ -185,7 +191,7 @@
     chunk = math.gcd(cache_rows, 1024)
 
     def attend(lap, carry):
-        k = lax.rem(lap, n)
+        k = lax.rem(2 * n - lap, n)
 
         @pl.when(k != 0)
         def _():
@@ -215,18 +221,39 @@
                 total = total + lane_fold(jnp.add, p)
                 o = o + jnp.dot(p.astype(BF16), cvs[c : c + chunk, hs], preferred_element_type=F32)
             l = jnp.sum(total, axis=1, keepdims=True)
-            numsend[k, :, hs] = o.astype(BF16)
+            numsend[k, h] = o.astype(BF16)
+
+            @pl.when(k != 0)
+            def _():
+                n_copy(k, h).start()
+
             stats = jnp.where(lane_s == 2 * h, m, jnp.where(lane_s == 2 * h + 1, l, stats))
         statsend[k] = stats.T[: statsend.shape[1]]
 
         @pl.when(k != 0)
         def _():
-            n_copy(k).start()
             s_copy(k).start()
 
         return carry
 
     lax.fori_loop(1, n + 1, attend, 0)
+
+    mate = tp + 1 - 2 * (tp % 2)
+
+    def a_copy(k, h):
+        return pltpu.make_async_remote_copy(
+            src_ref=attn_own.at[h], dst_ref=attn_recv.at[k, h], send_sem=a_ssem.at[k, h], recv_sem=a_rsem.at[k, h],
+            device_id={"tp": (tp + k) % t}, device_id_type=MESH)
+
+    def b_copy(k, h):
+        return pltpu.make_async_remote_copy(
+            src_ref=attn_recv.at[k, h], dst_ref=attn_recv.at[k + 1, h], send_sem=a_ssem.at[k + 1, h], recv_sem=a_rsem.at[k + 1, h],
+            device_id={"tp": mate}, device_id_type=MESH)
+
+    def mate_copy(h):
+        return pltpu.make_async_remote_copy(
+            src_ref=attn_own.at[h], dst_ref=attn_recv.at[1, h], send_sem=a_ssem.at[1, h], recv_sem=a_rsem.at[1, h],
+            device_id={"tp": mate}, device_id_type=MESH)
 
     stats = [statsend[0]]
     for k in range(1, n):
@@ -244,47 +271,35 @@
         weights += [f / l for f in fs]
     weights.append(jnp.zeros((128 - heads * n, rows), F32))
     cols = jnp.concatenate(weights, 0).T
-    for k in range(1, n):
-        n_copy(k).wait_recv()
-    for h in range(heads):
-        hs = slice(h * hd, (h + 1) * hd)
-        acc = numsend[0, :, hs].astype(F32) * cols[:, h * n : h * n + 1]
+    for h in range(heads):
         for k in range(1, n):
-            acc = acc + numrecv[k, :, hs].astype(F32) * cols[:, h * n + k : h * n + k + 1]
-        attn_own[:rows, hs] = acc.astype(BF16)
-
-    mate = tp + 1 - 2 * (tp % 2)
-
-    def a_copy(k):
-        return pltpu.make_async_remote_copy(
-            src_ref=attn_own, dst_ref=attn_recv.at[k], send_sem=a_ssem.at[k], recv_sem=a_rsem.at[k],
-            device_id={"tp": (tp + k) % t}, device_id_type=MESH)
-
-    def b_copy(k):
-        return pltpu.make_async_remote_copy(
-            src_ref=attn_recv.at[k], dst_ref=attn_recv.at[k + 1], send_sem=a_ssem.at[k + 1], recv_sem=a_rsem.at[k + 1],
-            device_id={"tp": mate}, device_id_type=MESH)
-
-    mate_copy = pltpu.make_async_remote_copy(
-        src_ref=attn_own, dst_ref=attn_recv.at[1], send_sem=a_ssem.at[1], recv_sem=a_rsem.at[1],
-        device_id={"tp": mate}, device_id_type=MESH)
-    for k in range(2, t, 2):
-        a_copy(k).start()
-    mate_copy.start()
+            n_copy(k, h).wait_recv()
+        acc = numsend[0, h].astype(F32) * cols[:, h * n : h * n + 1]
+        for k in range(1, n):
+            acc = acc + numrecv[k, h].astype(F32) * cols[:, h * n + k : h * n + k + 1]
+        attn_own[h, :rows, :] = acc.astype(BF16)
+        for k in range(2, t, 2):
+            a_copy(k, h).start()
+        mate_copy(h).start()
+
     loads[8].wait()
 
     def part(block, who):
+        block = jnp.concatenate([block[h] for h in range(heads)], 1)
         return jnp.dot(block, ows[pl.ds(pl.multiple_of(who * width, width), width), :], preferred_element_type=F32)
 
     acc = part(attn_own[...], tp)
-    mate_copy.wait_recv()
+    for h in range(heads):
+        mate_copy(h).wait_recv()
     acc = acc + part(attn_recv[1], mate)
     for k in range(2, t, 2):
-        a_copy(k).wait_recv()
-        b_copy(k).start()
+        for h in range(heads):
+            a_copy(k, h).wait_recv()
+            b_copy(k, h).start()
         acc = acc + part(attn_recv[k], (tp + t - k) % t)
     for k in range(2, t, 2):
-        b_copy(k).wait_recv()
+        for h in range(heads):
+            b_copy(k, h).wait_recv()
         acc = acc + part(attn_recv[k + 1], (mate + t - k) % t)
     out_p[...] = acc[:rows].astype(BF16)
     out_d[...] = acc[rows : rows + dec].astype(BF16)
@@ -294,12 +309,19 @@
     for k in range(1, n):
         q_copy(k).wait_send()
         t_copy(k).wait_send()
-        n_copy(k).wait_send()
+        for h in range(heads):
+            n_copy(k, h).wait_send()
         s_copy(k).wait_send()
-    mate_copy.wait_send()
-    for k in range(2, t, 2):
-        a_copy(k).wait_send()
-        b_copy(k).wait_send()
+    for h in range(heads):
+        mate_copy(h).wait_send()
+        for k in range(2, t, 2):
+            a_copy(k, h).wait_send()
+            b_copy(k, h).wait_send()
+
+
+def hand_over(*refs):
+    for src, dst in zip(refs[:4], refs[4:]):
+        dst[...] = src[...]
 
 
 def shards(
@@ -324,7 +346,7 @@
         return pltpu.VMEM(array.shape, array.dtype)
 
     dma = pltpu.SemaphoreType.DMA
-    return pl.pallas_call(
+    parts = pl.pallas_call(
         functools.partial(kernel, n, t, heads),
         out_shape=(
             jax.ShapeDtypeStruct((rows, cols), BF16),
@@ -332,7 +354,7 @@
             jax.ShapeDtypeStruct((rows, width), BF16),
             jax.ShapeDtypeStruct((rows, width), BF16),
         ),
-        in_specs=[any_space, vmem, vmem, any_space, any_space, any_space, vmem, vmem, any_space,
+        in_specs=[any_space, vmem, vmem, any_space, any_space, any_space, vmem, smem, any_space,
                   any_space, any_space, vmem, any_space, any_space, vmem, smem],
         out_specs=(vmem, vmem, any_space, any_space),
         scratch_shapes=[
@@ -341,12 +363,12 @@
             pltpu.VMEM((all_rows, depth), BF16),
             pltpu.VMEM((n, rows, width), BF16),
             pltpu.VMEM((n, 8, 128), F32),
-            pltpu.VMEM((n, rows, width), BF16),
-            pltpu.VMEM((n, rows, width), BF16),
+            pltpu.VMEM((n, heads, rows, width // heads), BF16),
+            pltpu.VMEM((n, heads, rows, width // heads), BF16),
             pltpu.VMEM((n, stat_rows, rows), F32),
             pltpu.VMEM((n, stat_rows, rows), F32),
-            pltpu.VMEM((all_rows, width), BF16),
-            pltpu.VMEM((t, all_rows, width), BF16),
+            pltpu.VMEM((heads, all_rows, width // heads), BF16),
+            pltpu.VMEM((t, heads, all_rows, width // heads), BF16),
             pltpu.VMEM((rows, width), BF16),
             pltpu.VMEM((rows, width), BF16),
             like(cache_gates),
@@ -354,16 +376,22 @@
             pltpu.VMEM((heads, rows), F32),
             pltpu.VMEM((heads, rows, cache_rows + rows), F32),
             dma((9,)), dma((2,)),
-            dma((n,)), dma((n,)), dma((n,)), dma((n,)), dma((n,)), dma((n,)), dma((n,)), dma((n,)),
-            dma((t,)), dma((t,)),
+            dma((n,)), dma((n,)), dma((n,)), dma((n,)), dma((n, heads)), dma((n, heads)), dma((n,)), dma((n,)),
+            dma((t, heads)), dma((t, heads)),
         ],
         compiler_params=pltpu.CompilerParams(
             collective_id=0, has_side_effects=True, vmem_limit_bytes=60 * 1024 * 1024),
     )(
         piece_tokens, dec_tokens, norm_gain.reshape(1, depth), query_weight, key_weight, value_weight,
-        forget_weight.T, forget_bias.reshape(heads, 1), out_weight, cache_keys, cache_values, cache_gates,
+        forget_weight.T, forget_bias, out_weight, cache_keys, cache_values, cache_gates,
         dec_keys, dec_values, dec_gates, dec_lengths,
     )
+    return pl.pallas_call(
+        hand_over,
+        out_shape=tuple(jax.ShapeDtypeStruct(p.shape, p.dtype) for p in parts),
+        in_specs=[vmem] * 4,
+        out_specs=(vmem,) * 4,
+    )(*parts)
 
 
 def solution(mesh):

time: 54.2 us -> 45.8 us (0.85)
  the two profiles are of different devices: /device:TPU:21 before, /device:TPU:0 now
where the time goes in v2:
time: 45.8 us; the launch traced here: 45.5 us
  Pallas kernels  44.9 us (98%)
  between operations  0.65 us (1%)
    pallas_call x1, Pallas kernels, shards(): pl.pallas_call(functools.partial(kernel, n, t, heads), out_shape=(jax.Sha...  43 us
    pallas_call x1, Pallas kernels, shards(): pl.pallas_call(hand_over, out_shape=tuple((jax.ShapeDtypeStruct(p.shape,...  1.86 us

profile of v2, /device:TPU:0, one launch (start us, length us, event | category | flops | bytes accessed | tf_op | source)
XLA Modules:
  0.0 45.5 jit_solution(7309597506555483592)
XLA Ops:
  0.6 43.0 %shard_map.183 = (bf16[256,512]{1,0:T(8,128)(2,1)}, bf16[4,512]{1,0:T(4,128)(2,1)}, bf16[256,256]{1,0:T(8,128)(2,1)}, bf16[256,256]{1,0:T(8,128)(2,1)}) custom-call(bf16[256,2048]{1,0:T(8,128)(2,1)} %piece_x.1, bf16[4,2048]{1,0:T(4,128)(2,1)} %dec_x.1, f32[1,2048]{1,0:T(1,128)} %bitcast.2, bf16[2048,256]{1,0:T(8,128)(2,1)} %qw.1, bf16[2048,256]{1,0:T(8,128)(2,1)} %kw.1, ...), custom_call_target="tpu_custom_call" | custom-call | tf_op jit(solution)/shard_map/pallas_call | solution.py:349
  43.7 1.9 %shard_map.184 = (bf16[256,512]{1,0:T(8,128)(2,1)}, bf16[4,512]{1,0:T(4,128)(2,1)}, bf16[256,256]{1,0:T(8,128)(2,1)}, bf16[256,256]{1,0:T(8,128)(2,1)}) custom-call(bf16[256,512]{1,0:T(8,128)(2,1)} %get-tuple-element.8.refs_0_, bf16[4,512]{1,0:T(4,128)(2,1)} %get-tuple-element.9.refs_1_, bf16[256,256]{1,0:T(8,128)(2,1)} %get-tuple-element.10.refs_2_, ...), custom_call_target="tpu_custom_call" | custom-call | tf_op jit(solution)/shard_map/pallas_call | solution.py:389
